TPU v7x, 32 devices: a whole 2x2x4 slice. The times are simulated.
32 devices in a mesh: ep: 16 (over z, y, x), tp: 2 (over core).
Axes of the slice: x: 2, y: 2, z: 4, core: 2. Of those that a mesh axis runs over, the one named last changes fastest.
Arguments:
- stream: bfloat16 [256, 2048], P('ep', 'tp'), may hold values from -6 to 6
- hidden_state: float32 [256, 2048], P('ep', 'tp'), may hold values from -6 to 6
- conv_state: bfloat16 [256, 3, 2048], P('ep', None, 'tp'), may hold values from -6 to 6
- first_gain: float32 [2048], P('tp'), may hold values from 0.1 to 1.9
- input_weight: bfloat16 [2048, 2048], P('tp', 'ep'), may hold values from -0.125 to 0.125
- branch_weight: bfloat16 [2048, 2048], P('tp', 'ep'), may hold values from -0.125 to 0.125
- conv_taps: bfloat16 [4, 2048], P(None, 'tp'), may hold values from -3 to 3
- recur_gate: bfloat16 [32, 64, 64], P('tp'), may hold values from -0.75 to 0.75
- input_gate: bfloat16 [32, 64, 64], P('tp'), may hold values from -0.75 to 0.75
- decay_logit: float32 [2048], P('tp'), may hold values from 1.5 to 8
- output_weight: bfloat16 [2048, 2048], P('tp', 'ep'), may hold values from -0.25 to 0.25
- second_gain: float32 [2048], P('tp'), may hold values from 0.1 to 1.9
- routes: int32 [256, 2], P('ep'), may hold values from 0 to 3, all different within a row; in each aligned block of 16 rows (0 to 15, 16 to 31, ...) at most 16 rows name the same one
- route_weight: float32 [256, 2], P('ep'), may hold values from 0.25 to 1
- expert_gate: bfloat16 [2048, 12288], P(None, ('ep', 'tp')), may hold values from -0.125 to 0.125
- expert_up: bfloat16 [2048, 12288], P(None, ('ep', 'tp')), may hold values from -0.125 to 0.125
- expert_down: bfloat16 [12288, 2048], P(('ep', 'tp')), may hold values from -0.21875 to 0.21875
Outputs:
- new_stream: bfloat16 [256, 2048], P('ep', 'tp')
- new_hidden: float32 [256, 2048], P('ep', 'tp')
- new_conv: bfloat16 [256, 3, 2048], P('ep', None, 'tp')
Inputs may be any that keep to these rules, and one draw needn't show every extreme that they name: `routes`: among the rows of one index of ep, no expert is named more than 16 times; in every draw some expert is named exactly 16 times by the rows of some index. Each row names different experts.
All inputs are finite; a program needn't handle non-finite values.
Results may differ from a plain program's by a relative error of at most 0.022.
Values may be sent and summed in bfloat16 or wider, within the bound.
A program may use at most 128 MiB of HBM per device.

v0:
```python
import jax
import jax.numpy as jnp
from jax import lax
from jax.sharding import PartitionSpec as P

EP_SPAN = 4


epsilon = 1e-06
decay_power = 8.0


def block_map(values, table):
    seq_count = values.shape[0]
    heads, inner_width, _ = table.shape
    split = values.reshape(seq_count, heads, inner_width)
    mapped = jnp.einsum("shi,hij->shj", split, table, preferred_element_type=jnp.float32)
    return mapped.reshape(seq_count, heads * inner_width)


def per_device(
    stream,
    hidden_state,
    conv_state,
    first_gain,
    input_weight,
    branch_weight,
    conv_taps,
    recur_gate,
    input_gate,
    decay_logit,
    output_weight,
    second_gain,
    routes,
    route_weight,
    expert_gate,
    expert_up,
    expert_down,
):
    seq_dev, half_width = stream.shape
    tp_count = lax.axis_size("tp")
    model_width = half_width * tp_count
    values = stream.astype(jnp.float32)
    square_sum = jnp.sum(values * values, axis=1)
    scaled = (values * first_gain).astype(jnp.bfloat16)
    paired = jnp.stack([input_weight, branch_weight], axis=1)
    partial_terms = jnp.einsum(
        "nd,dsc->nsc",
        lax.all_gather(scaled, "ep", axis=0, tiled=True),
        paired,
        preferred_element_type=jnp.float32,
    )
    partial_terms = lax.all_to_all(
        partial_terms.astype(jnp.bfloat16), "ep", split_axis=0, concat_axis=2, tiled=True
    ).astype(partial_terms.dtype)
    square_terms = jnp.broadcast_to(square_sum[:, None, None], (seq_dev, 1, tp_count))
    partial_terms, square_terms = (
        lax.psum_scatter(
            partial_terms.astype(jnp.bfloat16), "tp", scatter_dimension=2, tiled=True
        ).astype(jnp.float32),
        lax.psum_scatter(
            square_terms.astype(jnp.bfloat16), "tp", scatter_dimension=2, tiled=True
        ).astype(jnp.float32),
    )
    row_scale = lax.rsqrt(square_terms / model_width + epsilon)
    projected = (partial_terms * row_scale).astype(jnp.bfloat16)
    forward = projected[:, 0]
    branch = projected[:, 1]
    window = jnp.concatenate([conv_state, forward[:, None, :]], axis=1)
    new_conv = window[:, 1:]
    conv_out = jnp.einsum(
        "skc,kc->sc", window.astype(jnp.float32), conv_taps.astype(jnp.float32)
    ).astype(jnp.bfloat16)
    recur_open = jax.nn.sigmoid(block_map(conv_out, recur_gate))
    inward = jax.nn.sigmoid(block_map(conv_out, input_gate))
    log_decay = -decay_power * recur_open * jax.nn.softplus(-decay_logit)
    new_hidden = jnp.exp(log_decay) * hidden_state + jnp.sqrt(-jnp.expm1(2.0 * log_decay)) * (
        inward * conv_out.astype(jnp.float32)
    )
    mixed_rows = (jax.nn.gelu(branch.astype(jnp.float32)) * new_hidden).astype(jnp.bfloat16)
    out_terms = jnp.dot(
        lax.all_gather(mixed_rows, "ep", axis=0, tiled=True),
        output_weight,
        preferred_element_type=jnp.float32,
    )
    out_terms = lax.all_to_all(
        out_terms.astype(jnp.bfloat16), "ep", split_axis=0, concat_axis=1, tiled=True
    ).astype(out_terms.dtype)
    out_terms = lax.psum_scatter(
        out_terms.astype(jnp.bfloat16), "tp", scatter_dimension=1, tiled=True
    ).astype(jnp.float32)
    middle = (values + out_terms).astype(jnp.bfloat16)
    mid_values = middle.astype(jnp.float32)
    full_rows, full_gain = (
        lax.all_gather(middle, "tp", axis=1, tiled=True),
        lax.all_gather(second_gain.astype(jnp.bfloat16), "tp", axis=0, tiled=True).astype(
            second_gain.dtype
        ),
    )
    full_values = full_rows.astype(jnp.float32)
    mean_square = jnp.mean(full_values * full_values, axis=1, keepdims=True)
    normed = (full_values * lax.rsqrt(mean_square + epsilon) * full_gain).astype(jnp.bfloat16)
    experts = lax.axis_size("ep") // EP_SPAN
    top_count = routes.shape[1]
    capacity = max(2, 2 * seq_dev * top_count // experts)
    flat_routes = routes.reshape(-1)
    expert_hits = (flat_routes[:, None] == jnp.arange(experts, dtype=jnp.int32)[None, :]).astype(
        jnp.int32
    )
    slot_rank = jnp.sum((jnp.cumsum(expert_hits, axis=0) - expert_hits) * expert_hits, axis=1)
    target = flat_routes * capacity + slot_rank
    picking = target[:, None] == jnp.arange(experts * capacity, dtype=jnp.int32)[None, :]
    repeated = jnp.repeat(normed, top_count, axis=0)
    buffer = jnp.einsum(
        "ae,ad->ed", picking.astype(jnp.bfloat16), repeated, preferred_element_type=jnp.float32
    ).astype(jnp.bfloat16)
    buffer = buffer.reshape(experts, capacity, normed.shape[1])
    outgoing = jnp.repeat(buffer, EP_SPAN, axis=0)
    arrived = lax.all_to_all(outgoing, "ep", split_axis=0, concat_axis=0, tiled=True)
    sources, slot_count, _ = arrived.shape
    flat_rows = arrived.reshape(sources * slot_count, model_width)
    gate_act = jnp.dot(flat_rows, expert_gate, preferred_element_type=jnp.float32)
    upper = jnp.dot(flat_rows, expert_up, preferred_element_type=jnp.float32)
    inner_act = (jax.nn.silu(gate_act) * upper).astype(jnp.bfloat16)
    partial_value = jnp.dot(inner_act, expert_down, preferred_element_type=jnp.float32)
    partial_value = lax.psum_scatter(
        partial_value.astype(jnp.bfloat16), "tp", scatter_dimension=1, tiled=True
    ).astype(jnp.float32)
    partial_value = partial_value.reshape(sources, slot_count, half_width)
    returned = lax.all_to_all(
        partial_value.astype(jnp.bfloat16), "ep", split_axis=0, concat_axis=0, tiled=True
    ).astype(partial_value.dtype)
    summed = jnp.sum(returned.reshape(experts, EP_SPAN, capacity, half_width), axis=1).reshape(
        experts * capacity, half_width
    )
    picked = jnp.dot(
        picking.astype(jnp.float32),
        summed,
        precision=lax.Precision.HIGHEST,
        preferred_element_type=jnp.float32,
    )
    expert_mix = jnp.sum(
        picked.reshape(seq_dev, top_count, half_width) * route_weight[:, :, None], axis=1
    )
    new_stream = (mid_values + expert_mix).astype(jnp.bfloat16)
    return (new_stream, new_hidden, new_conv)


def solution(mesh):
    placed = (
        P("ep", "tp"),
        P("ep", "tp"),
        P("ep", None, "tp"),
        P("tp"),
        P("tp", "ep"),
        P("tp", "ep"),
        P(None, "tp"),
        P("tp", None, None),
        P("tp", None, None),
        P("tp"),
        P("tp", "ep"),
        P("tp"),
        P("ep", None),
        P("ep", None),
        P(None, ("ep", "tp")),
        P(None, ("ep", "tp")),
        P(("ep", "tp"), None),
    )
    return jax.shard_map(
        per_device,
        mesh=mesh,
        in_specs=placed,
        out_specs=(P("ep", "tp"), P("ep", "tp"), P("ep", None, "tp")),
        check_vma=False,
    )
```

profile of v0, /device:TPU:0, one launch (start us, length us, event | category | flops | bytes accessed | tf_op | source)
XLA Modules:
  0.0 214.5 jit_solution(16921557774375420503)
XLA Ops:
  7.2 1.0 fusion.26
  8.2 45.5 %all_gather.12 = bf16[256,1024]{1,0:T(8,128)(2,1)S(1)} all-gather(bf16[16,1024]{1,0:T(8,128)(2,1)S(1)} %get-tuple-element.6), channel_id=1, replica_groups=mesh['ep'=16,'tp'=2] {'ep'}, dimensions={0}, use_global_device_ids=true | all-gather | bytes 557056 | tf_op jit(solution)/shard_map/all_gather | solution.py:49
  53.7 1.4 convolution_convert_fusion.2
  55.1 0.8 copy.49
  55.9 3.5 %all-to-all-start = ((bf16[256,2,128]{2,1,0:T(2,128)(2,1)}), bf16[256,2,128]{2,1,0:T(2,128)(2,1)S(1)}, u32[]{:S(2)}, u32[]{:S(2)}) async-start(bf16[256,2,128]{2,1,0:T(2,128)(2,1)} %copy.49), calls=%async_computation | async-start | bytes 262144 | tf_op jit(solution)/shard_map/all_to_all | solution.py:53
  60.0 2.4 %all-reduce = bf16[16,1,2]{0,2,1:T(2,128)(2,1)S(1)} all-reduce(bf16[16,1,2]{0,2,1:T(2,128)(2,1)S(1)} %broadcast_in_dim.6), channel_id=3, replica_groups=mesh['ep'=16,'tp'=2] {'tp'}, use_global_device_ids=true, to_apply=%region_2.0.clone | all-reduce | flops 32 | bytes 128
  62.5 4.6 %all-to-all-done = bf16[256,2,128]{2,1,0:T(2,128)(2,1)S(1)} async-done(((bf16[256,2,128]{2,1,0:T(2,128)(2,1)}), bf16[256,2,128]{2,1,0:T(2,128)(2,1)S(1)}, u32[]{:S(2)}, u32[]{:S(2)}) %all-to-all-start) | async-done | bytes 131104 | tf_op jit(solution)/shard_map/all_to_all | solution.py:53
  68.8 4.0 %reduce-scatter.5.cloned.1.call-done = bf16[16,2,1024]{2,0,1:T(8,128)(2,1)} async-done(((bf16[16,2,2048]{2,0,1:T(8,128)(2,1)}), bf16[16,2,1024]{2,0,1:T(8,128)(2,1)}) %reduce-scatter.5.cloned.1.call-update) | async-done | bytes 65552 | tf_op jit(solution)/shard_map/reduce_scatter | solution.py:58
  72.8 0.9 multiply_convert_fusion
  74.7 0.7 fusion.34
  75.4 43.9 %all_gather.13 = bf16[256,1024]{1,0:T(8,128)(2,1)S(1)} all-gather(bf16[16,1024]{1,0:T(8,128)(2,1)S(1)} %get-tuple-element.3), channel_id=1, replica_groups=mesh['ep'=16,'tp'=2] {'ep'}, dimensions={0}, use_global_device_ids=true | all-gather | bytes 557056 | tf_op jit(solution)/shard_map/all_gather | solution.py:82
  119.3 0.9 convolution_convert_fusion.3
  120.2 3.5 %all-to-all-start.1 = ((bf16[16,16,128]{2,1,0:T(8,128)(2,1)}), bf16[16,16,128]{2,1,0:T(8,128)(2,1)S(1)}, u32[]{:S(2)}, u32[]{:S(2)}) async-start(bf16[16,16,128]{2,1,0:T(8,128)(2,1)} %bitcast.13), calls=%async_computation.2 | async-start | bytes 131072 | tf_op jit(solution)/shard_map/all_to_all | solution.py:86
  123.9 1.8 all_gather.15
  126.0 5.3 %all-to-all-done.1 = bf16[16,16,128]{2,1,0:T(8,128)(2,1)S(1)} async-done(((bf16[16,16,128]{2,1,0:T(8,128)(2,1)}), bf16[16,16,128]{2,1,0:T(8,128)(2,1)S(1)}, u32[]{:S(2)}, u32[]{:S(2)}) %all-to-all-start.1) | async-done | bytes 65568 | tf_op jit(solution)/shard_map/all_to_all | solution.py:86
  132.0 4.3 %reduce-scatter.7.cloned.1.call-done = bf16[16,1024]{1,0:T(8,128)(2,1)} async-done(((bf16[16,2048]{1,0:T(8,128)(2,1)}), bf16[16,1024]{1,0:T(8,128)(2,1)}) %reduce-scatter.7.cloned.1.call-update) | async-done | bytes 32784 | tf_op jit(solution)/shard_map/reduce_scatter | solution.py:89
  136.3 0.8 fusion.27
  137.1 1.9 all_gather.14
  139.8 33.4 %all_to_all.47 = bf16[16,16,2048]{2,1,0:T(8,128)(2,1)S(1)} all-to-all(bf16[16,16,2048]{2,1,0:T(8,128)(2,1)S(1)} %bitcast.72), channel_id=1, replica_groups=mesh['ep'=16,'tp'=2] {'ep'}, dimensions={0} | all-to-all | bytes 2097152 | tf_op jit(solution)/shard_map/all_to_all | solution.py:119
  173.2 0.7 fusion.47
  173.9 3.8 %convolution_convert_fusion = bf16[256,2048]{1,0:T(8,128)(2,1)} fusion(bf16[384,2048]{1,0:T(8,128)(2,1)S(1)} %copy-done, bf16[256,2048]{1,0:T(8,128)(2,1)S(1)} %bitcast.71, bf16[2048,384]{1,0:T(8,128)(2,1)} %param.32, f32[256,384]{1,0:T(8,128)S(1)} %fusion.47), kind=kOutput, calls=%fused_computation | convolution fusion | flops 806420480 | bytes 5636096 | tf_op jit(solution)/shard_map/dot_general | solution.py:125
  177.7 7.0 %reduce-scatter.9.cloned.1.call-done = bf16[256,1024]{1,0:T(8,128)(2,1)} async-done(((bf16[256,2048]{1,0:T(8,128)(2,1)}), bf16[256,1024]{1,0:T(8,128)(2,1)}) %reduce-scatter.9.cloned.1.call-update) | async-done | bytes 524304 | tf_op jit(solution)/shard_map/reduce_scatter | solution.py:126
  184.7 6.8 %all-to-all-start.3 = ((bf16[16,16,1024]{2,1,0:T(8,128)(2,1)}), bf16[16,16,1024]{2,1,0:T(8,128)(2,1)S(1)}, u32[]{:S(2)}, u32[]{:S(2)}) async-start(bf16[16,16,1024]{2,1,0:T(8,128)(2,1)} %bitcast.75), calls=%async_computation.6 | async-start | bytes 1048576 | tf_op jit(solution)/shard_map/all_to_all | solution.py:130
  192.3 14.6 %all-to-all-done.3 = bf16[16,16,1024]{2,1,0:T(8,128)(2,1)S(1)} async-done(((bf16[16,16,1024]{2,1,0:T(8,128)(2,1)}), bf16[16,16,1024]{2,1,0:T(8,128)(2,1)S(1)}, u32[]{:S(2)}, u32[]{:S(2)}) %all-to-all-start.3) | async-done | bytes 524320 | tf_op jit(solution)/shard_map/all_to_all | solution.py:130
  (73 shorter events, 6.8 us)
Async XLA Ops:
  7.2 166.7 %copy-start = (bf16[384,2048]{1,0:T(8,128)(2,1)S(1)}, bf16[384,2048]{1,0:T(8,128)(2,1)}, u32[]{:S(2)}) copy-start(bf16[384,2048]{1,0:T(8,128)(2,1)} %param.33) | copy-start | bytes 4718596
  7.2 52.2 %copy-start.13 = (u32[32]{0:T(128)S(1)}, u32[32]{0:T(128)}, u32[]{:S(2)}) copy-start(u32[32]{0:T(128)} %constant.37) | copy-start | bytes 388
  7.2 55.3 %copy-start.9 = (f32[1024]{0:T(1024)S(1)}, f32[1024]{0:T(1024)}, u32[]{:S(2)}) copy-start(f32[1024]{0:T(1024)} %param.26) | copy-start | bytes 12292
  8.2 60.4 %copy-start.7 = (s32[16,2]{0,1:T(2,128)S(1)}, s32[16,2]{0,1:T(2,128)}, u32[]{:S(2)}) copy-start(s32[16,2]{0,1:T(2,128)} %param.29) | copy-start | bytes 388
  8.2 60.6 %copy-start.6 = (bf16[4,1024]{1,0:T(4,128)(2,1)S(1)}, bf16[4,1024]{1,0:T(4,128)(2,1)}, u32[]{:S(2)}) copy-start(bf16[4,1024]{1,0:T(4,128)(2,1)} %param.23) | copy-start | bytes 24580
  53.7 20.1 %copy-start.2 = (bf16[16,3,1024]{2,0,1:T(8,128)(2,1)S(1)}, bf16[16,3,1024]{2,0,1:T(8,128)(2,1)}, u32[]{:S(2)}) copy-start(bf16[16,3,1024]{2,0,1:T(8,128)(2,1)} %param.19) | copy-start | bytes 294916
  53.7 20.2 %copy-start.11 = (bf16[16,64,64]{2,1,0:T(8,128)(2,1)S(1)}, bf16[16,64,64]{2,1,0:T(8,128)(2,1)}, u32[]{:S(2)}) copy-start(bf16[16,64,64]{2,1,0:T(8,128)(2,1)} %param.24) | copy-start | bytes 393220
  55.1 19.2 %copy-start.12 = (bf16[16,64,64]{2,1,0:T(8,128)(2,1)S(1)}, bf16[16,64,64]{2,1,0:T(8,128)(2,1)}, u32[]{:S(2)}) copy-start(bf16[16,64,64]{2,1,0:T(8,128)(2,1)} %param.25) | copy-start | bytes 393220
  55.9 11.3 %all-to-all-start = ((bf16[256,2,128]{2,1,0:T(2,128)(2,1)}), bf16[256,2,128]{2,1,0:T(2,128)(2,1)S(1)}, u32[]{:S(2)}, u32[]{:S(2)}) async-start(bf16[256,2,128]{2,1,0:T(2,128)(2,1)} %copy.49), calls=%async_computation | async-start | bytes 262144 | tf_op jit(solution)/shard_map/all_to_all | solution.py:53
  59.4 13.4 %reduce-scatter.5.cloned.1.call-start = ((), (), s32[]{:S(2)}) async-start(), calls=%async_computation.7 | async-start | bytes 196608 | tf_op jit(solution)/shard_map/reduce_scatter | solution.py:58
  67.9 6.8 %copy-start.5 = (f32[16,1024]{1,0:T(8,128)S(1)}, f32[16,1024]{1,0:T(8,128)}, u32[]{:S(2)}) copy-start(f32[16,1024]{1,0:T(8,128)} %param.18) | copy-start | bytes 196612
  73.9 45.4 %copy-start.3 = (bf16[1024,128]{1,0:T(8,128)(2,1)S(1)}, bf16[1024,128]{1,0:T(8,128)(2,1)}, u32[]{:S(2)}) copy-start(bf16[1024,128]{1,0:T(8,128)(2,1)} %param.27) | copy-start | bytes 786436
  74.3 49.6 %copy-start.8 = (f32[1024]{0:T(1024)S(1)}, f32[1024]{0:T(1024)}, u32[]{:S(2)}) copy-start(f32[1024]{0:T(1024)} %param.28) | copy-start | bytes 12292
  74.3 62.0 %copy-start.4 = (bf16[16,1024]{1,0:T(8,128)(2,1)S(1)}, bf16[16,1024]{1,0:T(8,128)(2,1)}, u32[]{:S(2)}) copy-start(bf16[16,1024]{1,0:T(8,128)(2,1)} %param.17) | copy-start | bytes 98308
  120.2 11.0 %all-to-all-start.1 = ((bf16[16,16,128]{2,1,0:T(8,128)(2,1)}), bf16[16,16,128]{2,1,0:T(8,128)(2,1)S(1)}, u32[]{:S(2)}, u32[]{:S(2)}) async-start(bf16[16,16,128]{2,1,0:T(8,128)(2,1)} %bitcast.13), calls=%async_computation.2 | async-start | bytes 131072 | tf_op jit(solution)/shard_map/all_to_all | solution.py:86
  123.8 12.6 %reduce-scatter.7.cloned.1.call-start = ((), (), s32[]{:S(2)}) async-start(), calls=%async_computation.8 | async-start | bytes 98304 | tf_op jit(solution)/shard_map/reduce_scatter | solution.py:89
  131.9 52.8 %reduce-scatter.9.cloned.1.call-start = ((), (), s32[]{:S(2)}) async-start(), calls=%async_computation.9 | async-start | bytes 1572864 | tf_op jit(solution)/shard_map/reduce_scatter | solution.py:126
  139.7 33.5 %copy-start.1 = (bf16[2048,384]{1,0:T(8,128)(2,1)S(1)}, bf16[2048,384]{1,0:T(8,128)(2,1)}, u32[]{:S(2)}) copy-start(bf16[2048,384]{1,0:T(8,128)(2,1)} %param.31) | copy-start | bytes 4718596
  177.7 29.4 %copy-start.10 = (f32[16,2]{0,1:T(2,128)S(1)}, f32[16,2]{0,1:T(2,128)}, u32[]{:S(2)}) copy-start(f32[16,2]{0,1:T(2,128)} %param.30) | copy-start | bytes 388
  184.7 22.3 %all-to-all-start.3 = ((bf16[16,16,1024]{2,1,0:T(8,128)(2,1)}), bf16[16,16,1024]{2,1,0:T(8,128)(2,1)S(1)}, u32[]{:S(2)}, u32[]{:S(2)}) async-start(bf16[16,16,1024]{2,1,0:T(8,128)(2,1)} %bitcast.75), calls=%async_computation.6 | async-start | bytes 1048576 | tf_op jit(solution)/shard_map/all_to_all | solution.py:130
Sparse Core Ops, SparseCore 0:
  68.0 4.7 reduce-scatter.4
  132.0 4.2 reduce-scatter.6
  177.9 6.7 reduce-scatter.8
where the time goes:
time: 215 us; the launch traced here: 214 us
  blocking collectives  129 us (60%)
  waiting for transfers between devices  39.9 us (19%)
  between operations  14.1 us (7%)
  starting transfers between devices  13.9 us (6%)
  matrix products  7.82 us (4%)
  other arithmetic  6.06 us (3%)
  local copies, waits for them, and re-layouts  3.79 us (2%)
    all_gather x1, blocking collectives, per_device(): lax.all_gather(scaled, 'ep', axis=0, tiled=True)  45.5 us
    all_gather x1, blocking collectives, per_device(): lax.all_gather(mixed_rows, 'ep', axis=0, tiled=True)  43.9 us
    all_to_all x1, blocking collectives, per_device(): lax.all_to_all(outgoing, 'ep', split_axis=0, concat_axis=0, tiled=True)  33.4 us
    all_to_all x1, waiting for transfers between devices, per_device(): lax.all_to_all(partial_value.astype(jnp.bfloat16), 'ep', split_axis=0, co...  14.6 us
    reduce_scatter x1, waiting for transfers between devices, per_device(): lax.psum_scatter(partial_value.astype(jnp.bfloat16), 'tp', scatter_dimens...  6.96 us
    all_to_all x1, starting transfers between devices, per_device(): lax.all_to_all(partial_value.astype(jnp.bfloat16), 'ep', split_axis=0, co...  6.79 us
    all_to_all x1, waiting for transfers between devices, per_device(): lax.all_to_all(out_terms.astype(jnp.bfloat16), 'ep', split_axis=0, concat...  5.29 us
    all_to_all x1, waiting for transfers between devices, per_device(): lax.all_to_all(partial_terms.astype(jnp.bfloat16), 'ep', split_axis=0, co...  4.65 us
  transfers between devices with their start and end apart: 6, of which 6 were waited for; matrix products, arithmetic and copies ran while one was open for 1% of the time, Pallas kernels for 0%

commit v1 on v0

v1 whole, which is shorter than its diff:
```python
import functools

import jax
import jax.numpy as jnp
from jax import lax
from jax.experimental import pallas as pl
from jax.experimental.pallas import tpu as pltpu
from jax.sharding import PartitionSpec as P

EP_SPAN = 4
PLANE = 4
MESH = pl.DeviceIdType.MESH

epsilon = 1e-06
decay_power = 8.0
bf16 = jnp.bfloat16
f32 = jnp.float32


def kernel(
    n,
    stream,
    hidden,
    conv,
    gain1,
    win_hbm,
    wbr_hbm,
    taps,
    rgate,
    igate,
    decay,
    wout_hbm,
    gain2,
    routes,
    rweight,
    wg_hbm,
    wu_hbm,
    wd_hbm,
    new_stream,
    new_hidden,
    new_conv,
    win,
    wbr,
    wout,
    wg,
    wu,
    wd,
    rdiag,
    idiag,
    wx,
    x1,
    x2,
    x3,
    xp,
    sq,
    pair1s,
    pair1r,
    fin1,
    y1,
    pair2s,
    pair2r,
    fin2,
    y2,
    inner,
    pair3s,
    pair3r,
    keep,
    sums,
    r1,
    t2,
    r2,
    u3,
    r3,
    load_sem,
    wx_s,
    wx_r,
    sq_s,
    sq_r,
    ag_s,
    ag_r,
    pair_s,
    pair_r,
    y_s,
    y_r,
    xp_s,
    xp_r,
    rs_s,
    rs_r,
):
    e = lax.axis_index("ep")
    t = lax.axis_index("tp")
    rows, half = stream.shape
    zn = n // PLANE
    hn = n // 2
    cols = win.shape[1]
    z, low = e // PLANE, e % PLANE
    lx, ly = low % 2, low // 2
    ex = e + 1 - 2 * lx
    ey = e + 2 - 4 * ly
    other = 1 - t
    pending = []

    def rcopy(src, dst, ssem, rsem, ep, tp):
        return pltpu.make_async_remote_copy(
            src_ref=src,
            dst_ref=dst,
            send_sem=ssem,
            recv_sem=rsem,
            device_id=(ep, tp),
            device_id_type=MESH,
        )

    def send(*args):
        c = rcopy(*args)
        c.start()
        pending.append(c)
        return c

    loads = []
    for i, (a, b) in enumerate(
        ((win_hbm, win), (wbr_hbm, wbr), (wout_hbm, wout), (wg_hbm, wg), (wu_hbm, wu), (wd_hbm, wd))
    ):
        c = pltpu.make_async_copy(a, b, load_sem.at[i])
        c.start()
        loads.append(c)

    def gather(buf, p, after=None):
        s, r = ag_s.at[p], ag_r.at[p]
        at = [lax.rem(z - k + zn, zn) for k in range(zn)]
        zc = [None] * zn
        for k in range(1, zn):
            target = lax.rem(e + PLANE * k, n)
            zc[k] = send(buf.at[0, z], buf.at[0, z], s.at[0, k], r.at[0, k], target, t)
        xc, yc, dc = [None] * zn, [None] * zn, [None] * zn

        def diagonal(k):
            if k % 2 == 0:
                xc[k].wait_recv()
                dc[k] = send(buf.at[1, at[k]], buf.at[3, at[k]], s.at[3, k], r.at[3, k], ey, t)
                if after:
                    after(1, at[k], k)
            else:
                yc[k].wait_recv()
                dc[k] = send(buf.at[2, at[k]], buf.at[3, at[k]], s.at[3, k], r.at[3, k], ex, t)
                if after:
                    after(2, at[k], k)

        for k in range(zn):
            if k:
                zc[k].wait_recv()
            xc[k] = send(buf.at[0, at[k]], buf.at[1, at[k]], s.at[1, k], r.at[1, k], ex, t)
            yc[k] = send(buf.at[0, at[k]], buf.at[2, at[k]], s.at[2, k], r.at[2, k], ey, t)
            if after:
                after(0, at[k], k)
            if k:
                diagonal(k - 1)
        diagonal(zn - 1)
        for k in range(zn):
            if k % 2 == 0:
                yc[k].wait_recv()
                if after:
                    after(2, at[k], k)
            else:
                xc[k].wait_recv()
                if after:
                    after(1, at[k], k)
        for k in range(zn):
            dc[k].wait_recv()
            if after:
                after(3, at[k], k)

    values = stream[...].astype(f32)
    x1[0, z] = (values * gain1[...]).astype(bf16)
    sq[0, 0] = jnp.broadcast_to(jnp.sum(values * values, axis=1, keepdims=True), (rows, 128))
    lane = lax.broadcasted_iota(jnp.int32, (rows, 128), 1)
    wrow = jnp.zeros((rows, 128), f32)
    for k in range(routes.shape[1]):
        wrow += jnp.where(lane == routes[:, k : k + 1], rweight[:, k : k + 1], 0.0)
    wx[0, z] = wrow

    def weights_out():
        out = []
        for q in range(PLANE):
            tx = lax.rem(lx + q % 2, 2)
            ty = lax.rem(ly + q // 2, 2)
            for k in range(zn):
                if q == 0 and k == 0:
                    continue
                target = lax.rem(z + k, zn) * PLANE + 2 * ty + tx
                out.append(send(wx.at[0, z], wx.at[q, z], wx_s.at[q, k], wx_r.at[q, k], target, t))
        return out

    sq1 = send(sq.at[0, 0], sq.at[0, 1], sq_s.at[0], sq_r.at[0], e, other)

    def prepare():
        rdiag[...] = jnp.zeros_like(rdiag)
        idiag[...] = jnp.zeros_like(idiag)
        heads, w, _ = rgate.shape
        per = rdiag.shape[1] // w
        for h in range(heads):
            g, o = h // per, (h % per) * w
            rdiag[g, o : o + w, o : o + w] = rgate[h]
            idiag[g, o : o + w, o : o + w] = igate[h]

    gather(x1, 0)
    wxc = weights_out()
    prepare()

    loads[0].wait()
    loads[1].wait()

    def project(x, weights, pairs, pairr, fin, y, p):
        m = len(weights)

        def part(side):
            lhs = x[pl.ds(2 * side, 2)].reshape(hn * rows, half)
            return [jnp.dot(lhs, w[...], preferred_element_type=f32) for w in weights]

        away = part(other)
        for i in range(m):
            pairs[i] = away[i].astype(bf16)
        pc = send(pairs, pairr, pair_s.at[p], pair_r.at[p], e, other)
        mine = part(t)
        pc.wait_recv()
        for i in range(m):
            total = mine[i] + pairr[i].astype(f32)
            fin[:, i] = total.astype(bf16).reshape(hn, rows, cols)
        owner = e // hn
        slot = e - owner * hn
        own = jnp.logical_and(t == 0, owner == 0)
        ycs = []
        for i in range(2):
            for zz in range(zn):
                tx = lax.rem(lx + i, 2)
                ty = lax.rem(ly + t, 2)
                k = lax.rem(z + zz, zn)
                target = k * PLANE + 2 * ty + tx
                b = i * zn + k
                c = rcopy(
                    fin.at[b], y.at[slot], y_s.at[p, i * zn + zz], y_r.at[p, slot], target, owner
                )
                if i == 0 and zz == 0:

                    @pl.when(jnp.logical_not(own))
                    def _():
                        c.start()

                    @pl.when(own)
                    def _():
                        y[slot] = fin[b]
                else:
                    c.start()
                ycs.append(c)
        for j in range(hn):
            c = rcopy(fin.at[0], y.at[j], y_s.at[p, 0], y_r.at[p, j], e, other)

            @pl.when(jnp.logical_not(jnp.logical_and(own, slot == j)))
            def _():
                c.wait_recv()

        def finish():
            for i, c in enumerate(ycs):
                if i == 0:

                    @pl.when(jnp.logical_not(own))
                    def _():
                        c.wait_send()
                else:
                    c.wait_send()

        return [
            jnp.concatenate([y[j, i] for j in range(hn)], axis=1).astype(f32) for i in range(m)
        ], finish

    (fsum, bsum), finish1 = project(x1, (win, wbr), pair1s, pair1r, fin1, y1, 0)
    sq1.wait_recv()
    mean = (sq[0, 0][:, :1] + sq[0, 1][:, :1]) / (2 * half)
    scale = lax.rsqrt(mean + epsilon)
    forward = (fsum * scale).astype(bf16)
    branch = (bsum * scale).astype(bf16).astype(f32)

    width = taps.shape[0]
    acc = forward.astype(f32) * taps[width - 1 : width, :].astype(f32)
    for k in range(width - 1):
        acc += conv[:, k * half : (k + 1) * half].astype(f32) * taps[k : k + 1, :].astype(f32)
    conv_out = acc.astype(bf16)
    if width > 2:
        new_conv[:, : (width - 2) * half] = conv[:, half : (width - 1) * half]
    new_conv[:, (width - 2) * half :] = forward
    groups, gw, _ = rdiag.shape

    def block_map(table):
        return jnp.concatenate(
            [
                jnp.dot(
                    conv_out[:, g * gw : (g + 1) * gw], table[g], preferred_element_type=f32
                )
                for g in range(groups)
            ],
            axis=1,
        )

    recur_open = jax.nn.sigmoid(block_map(rdiag))
    inward = jax.nn.sigmoid(block_map(idiag))
    neg = -decay[...]
    soft = jnp.maximum(neg, 0.0) + jnp.log1p(jnp.exp(-jnp.abs(neg)))
    u = decay_power * recur_open * soft
    th = jnp.tanh(u)
    state = jnp.exp(-u) * hidden[...] + jnp.sqrt(2.0 * th / (1.0 + th)) * (
        inward * conv_out.astype(f32)
    )
    new_hidden[...] = state
    gelu = 0.5 * branch * (1.0 + jnp.tanh(0.7978845608028654 * (branch + 0.044715 * branch * branch * branch)))
    x2[0, z] = (gelu * state).astype(bf16)

    gather(x2, 1)
    loads[2].wait()
    (osum,), finish2 = project(x2, (wout,), pair2s, pair2r, fin2, y2, 1)
    middle = (values + osum).astype(bf16).astype(f32)
    sq[1, 0] = jnp.broadcast_to(jnp.sum(middle * middle, axis=1, keepdims=True), (rows, 128))
    sq2 = send(sq.at[1, 0], sq.at[1, 1], sq_s.at[1], sq_r.at[1], e, other)
    sq2.wait_recv()
    mean = (sq[1, 0][:, :1] + sq[1, 1][:, :1]) / (2 * half)
    x3[0, z] = (middle * lax.rsqrt(mean + epsilon) * gain2[...]).astype(bf16)

    xpc = []

    def relay(q, at, k):
        xpc.append(
            send(x3.at[q, at], xp.at[q, at], xp_s.at[q, k], xp_r.at[q, k], e, other)
        )

    gather(x3, 2, relay)
    loads[3].wait()
    loads[4].wait()
    for c in xpc:
        c.wait_recv()

    mrows = zn * rows
    here, there = pl.ds(pl.multiple_of(t * half, half), half), pl.ds(
        pl.multiple_of(other * half, half), half
    )
    per = EP_SPAN if n >= 2 * EP_SPAN or n == EP_SPAN else n
    expert = e // per
    for c in wxc:
        c.wait_recv()
    loads[5].wait()

    def each(count, body):
        if count == 1:
            body(0)
        else:
            pl.loop(0, count)(body)

    step = min(PLANE, max(1, 256 // mrows))

    def experts(c):
        qs = pl.ds(c * step, step)
        a = x3[qs].reshape(step * mrows, half)
        b = xp[qs].reshape(step * mrows, half)
        gate = jnp.dot(a, wg[here, :], preferred_element_type=f32) + jnp.dot(
            b, wg[there, :], preferred_element_type=f32
        )
        upper = jnp.dot(a, wu[here, :], preferred_element_type=f32) + jnp.dot(
            b, wu[there, :], preferred_element_type=f32
        )
        inner[qs] = (jax.nn.silu(gate) * upper).astype(bf16).reshape(step, mrows, gate.shape[1])

    each(PLANE // step, experts)

    def row_weights(qs):
        full = wx[qs].reshape(step * mrows, 128)
        lanes = lax.broadcasted_iota(jnp.int32, full.shape, 1)
        return jnp.sum(jnp.where(lanes == expert, full, 0.0), axis=1, keepdims=True)

    hw = half // 2

    def store(ref, qs, lanes):
        def run():
            act = inner[qs].reshape(step * mrows, inner.shape[2])
            out = jnp.dot(act, wd[:, lanes], preferred_element_type=f32) * row_weights(qs)
            for i in range(2):
                ref[i, qs] = (
                    out[:, i * hw : (i + 1) * hw].astype(ref.dtype).reshape(step, zn, rows, hw)
                )

        return run

    each(PLANE // step, lambda c: store(pair3s, pl.ds(c * step, step), there)())
    pc = send(pair3s, pair3r, pair_s.at[2], pair_r.at[2], e, other)
    each(PLANE // step, lambda c: store(keep, pl.ds(c * step, step), here)())
    pc.wait_recv()

    def total(i, q):
        return keep[i, q] + pair3r[i, q].astype(f32)

    first = (1, 2)
    rc = [[None, None], [None, None]]
    peers = (ex, ey)
    for i in range(2):
        sums[i, 1] = total(i, 3).astype(bf16)
        rc[i][1] = send(sums.at[i, 1], r1.at[i, 1], rs_s.at[0, i, 1], rs_r.at[0, i, 1], peers[i], t)
    for i in range(2):
        sums[i, 0] = total(i, first[i]).astype(bf16)
        rc[i][0] = send(sums.at[i, 0], r1.at[i, 0], rs_s.at[0, i, 0], rs_r.at[0, i, 0], peers[i], t)
    sc = [None, None]
    for i in range(2):
        rc[i][1].wait_recv()
        t2[i] = (total(i, first[1 - i]) + r1[i, 1].astype(f32)).astype(bf16)
        sc[i] = send(t2.at[i], r2.at[i], rs_s.at[1, i, 0], rs_r.at[1, i, 0], peers[1 - i], t)
    for i in range(2):
        rc[i][0].wait_recv()
        sc[i].wait_recv()
        keep[i, 0] = total(i, 0) + r1[i, 0].astype(f32) + r2[i].astype(f32)
        u3[:, :, i * hw : (i + 1) * hw] = keep[i, 0].astype(bf16)
    zc = []
    for k in range(1, zn):
        dest = lax.rem(z + k, zn)
        zc.append(
            send(u3.at[dest], r3.at[k], rs_s.at[2, 0, k], rs_r.at[2, 0, k], dest * PLANE + low, t)
        )
    mix = jnp.concatenate([keep[0, 0, z], keep[1, 0, z]], axis=1)
    for k in range(1, zn):
        zc[k - 1].wait_recv()
        mix += r3[k].astype(f32)
    new_stream[...] = (middle + mix).astype(bf16)
    finish1()
    finish2()
    for c in pending:
        c.wait_send()


def per_device(
    stream,
    hidden_state,
    conv_state,
    first_gain,
    input_weight,
    branch_weight,
    conv_taps,
    recur_gate,
    input_gate,
    decay_logit,
    output_weight,
    second_gain,
    routes,
    route_weight,
    expert_gate,
    expert_up,
    expert_down,
):
    n = lax.axis_size("ep")
    rows, half = stream.shape
    past = conv_state.shape[1]
    zn, hn = n // PLANE, n // 2
    cols = input_weight.shape[1]
    hidden_units = expert_gate.shape[1]
    heads, block, _ = recur_gate.shape
    gw = max(128, block)
    hw = half // 2
    dma = pltpu.SemaphoreType.DMA
    vm = pltpu.VMEM
    any_spec = pl.BlockSpec(memory_space=pl.ANY)
    vspec = pl.BlockSpec(memory_space=pltpu.VMEM)
    scratch = [
        vm(input_weight.shape, bf16),
        vm(branch_weight.shape, bf16),
        vm(output_weight.shape, bf16),
        vm(expert_gate.shape, bf16),
        vm(expert_up.shape, bf16),
        vm(expert_down.shape, bf16),
        vm((heads * block // gw, gw, gw), bf16),
        vm((heads * block // gw, gw, gw), bf16),
        vm((PLANE, zn, rows, 128), f32),
        vm((PLANE, zn, rows, half), bf16),
        vm((PLANE, zn, rows, half), bf16),
        vm((PLANE, zn, rows, half), bf16),
        vm((PLANE, zn, rows, half), bf16),
        vm((2, 2, rows, 128), f32),
        vm((2, hn * rows, cols), bf16),
        vm((2, hn * rows, cols), bf16),
        vm((hn, 2, rows, cols), bf16),
        vm((hn, 2, rows, cols), bf16),
        vm((1, hn * rows, cols), bf16),
        vm((1, hn * rows, cols), bf16),
        vm((hn, 1, rows, cols), bf16),
        vm((hn, 1, rows, cols), bf16),
        vm((PLANE, zn * rows, hidden_units), bf16),
        vm((2, PLANE, zn, rows, hw), bf16),
        vm((2, PLANE, zn, rows, hw), bf16),
        vm((2, PLANE, zn, rows, hw), f32),
        vm((2, 2, zn, rows, hw), bf16),
        vm((2, 2, zn, rows, hw), bf16),
        vm((2, zn, rows, hw), bf16),
        vm((2, zn, rows, hw), bf16),
        vm((zn, rows, half), bf16),
        vm((zn, rows, half), bf16),
        dma((6,)),
        dma((PLANE, zn)),
        dma((PLANE, zn)),
        dma((2,)),
        dma((2,)),
        dma((3, PLANE, zn)),
        dma((3, PLANE, zn)),
        dma((3,)),
        dma((3,)),
        dma((2, hn)),
        dma((2, hn)),
        dma((PLANE, zn)),
        dma((PLANE, zn)),
        dma((3, 2, max(2, zn))),
        dma((3, 2, max(2, zn))),
    ]
    a, v = any_spec, vspec
    new_stream, new_hidden, new_conv = pl.pallas_call(
        functools.partial(kernel, n),
        name="layer",
        out_shape=(
            jax.ShapeDtypeStruct(stream.shape, bf16),
            jax.ShapeDtypeStruct(stream.shape, f32),
            jax.ShapeDtypeStruct((rows, past * half), bf16),
        ),
        in_specs=[v, v, v, v, a, a, v, v, v, v, a, v, v, v, a, a, a],
        out_specs=(v, v, v),
        scratch_shapes=scratch,
        compiler_params=pltpu.CompilerParams(
            has_side_effects=True, vmem_limit_bytes=60 * 1024 * 1024
        ),
    )(
        stream,
        hidden_state,
        conv_state.reshape(rows, past * half),
        first_gain.reshape(1, half),
        input_weight,
        branch_weight,
        conv_taps,
        recur_gate,
        input_gate,
        decay_logit.reshape(1, half),
        output_weight,
        second_gain.reshape(1, half),
        routes,
        route_weight,
        expert_gate,
        expert_up,
        expert_down,
    )
    return new_stream, new_hidden, new_conv.reshape(rows, past, half)


def solution(mesh):
    placed = (
        P("ep", "tp"),
        P("ep", "tp"),
        P("ep", None, "tp"),
        P("tp"),
        P("tp", "ep"),
        P("tp", "ep"),
        P(None, "tp"),
        P("tp", None, None),
        P("tp", None, None),
        P("tp"),
        P("tp", "ep"),
        P("tp"),
        P("ep", None),
        P("ep", None),
        P(None, ("ep", "tp")),
        P(None, ("ep", "tp")),
        P(("ep", "tp"), None),
    )
    return jax.shard_map(
        per_device,
        mesh=mesh,
        in_specs=placed,
        out_specs=(P("ep", "tp"), P("ep", "tp"), P("ep", None, "tp")),
        check_vma=False,
    )
```

time: 215 us -> 88.2 us (0.41)
  blocking collectives: 129 us -> 0 us
  Pallas kernels: 0 us -> 78.6 us
  waiting for transfers between devices: 39.9 us -> 0 us
  starting transfers between devices: 13.9 us -> 0 us
  between operations: 14.1 us -> 0.64 us
  matrix products: 7.82 us -> 0 us
  other arithmetic: 6.06 us -> 0 us
  local copies, waits for them, and re-layouts: 3.79 us -> 8.63 us
    all_gather x4 -> x0, blocking collectives: 93.1 us -> none  [the longest x1 45.5 us: per_device(): lax.all_gather(scaled, 'ep', axis=0, tiled=True)]
    pallas_call x0 -> x1, Pallas kernels: none -> 78.6 us  [per_device(): pl.pallas_call(functools.partial(kernel, n), name='layer', out_shape=(jax...]
    all_to_all x1 -> x0, blocking collectives: 33.4 us -> none  [per_device(): lax.all_to_all(outgoing, 'ep', split_axis=0, concat_axis=0, tiled=True)]
    all_to_all x3 -> x0, waiting for transfers between devices: 24.6 us -> none  [the longest x1 14.6 us: per_device(): lax.all_to_all(partial_value.astype(jnp.bfloat16), 'ep', split_axis=0, co...]
    reduce_scatter x3 -> x0, waiting for transfers between devices: 15.3 us -> none  [the longest x1 6.96 us: per_device(): lax.psum_scatter(partial_value.astype(jnp.bfloat16), 'tp', scatter_dimens...]
    all_to_all x3 -> x0, starting transfers between devices: 13.8 us -> none  [the longest x1 6.79 us: per_device(): lax.all_to_all(partial_value.astype(jnp.bfloat16), 'ep', split_axis=0, co...]
    dot_general x8 -> x0, matrix products: 7.82 us -> none  [the longest x1 3.8 us: per_device(): jnp.dot(inner_act, expert_down, preferred_element_type=jnp.float32)]
    unnamed x30 -> x4, local copies, waits for them, and re-layouts: 0.75 us -> 5.55 us
  transfers between devices with their start and end apart: 6 -> 0, of which waited for: 6 -> 0; matrix products, arithmetic and copies ran while one was open for 1% -> 0% of each run, Pallas kernels for 0% -> 0%
where the time goes in v1:
time: 88.2 us; the launch traced here: 87.9 us
  Pallas kernels  78.6 us (89%)
  local copies, waits for them, and re-layouts  8.63 us (10%)
    pallas_call x1, Pallas kernels, per_device(): pl.pallas_call(functools.partial(kernel, n), name='layer', out_shape=(jax...  78.6 us
    unnamed x4, local copies, waits for them, and re-layouts  5.55 us

profile of v1, /device:TPU:0, one launch (start us, length us, event | category | flops | bytes accessed | tf_op | source)
XLA Modules:
  0.0 87.9 jit_solution(11631470208531504386)
XLA Ops:
  0.6 1.4 %copy.25.routes = s32[16,2]{1,0:T(8,128)} copy(s32[16,2]{0,1:T(2,128)} %param.29) | data formatting | bytes 256 | tf_op args[12]
  2.0 1.4 %copy.26.rweight = f32[16,2]{1,0:T(8,128)} copy(f32[16,2]{0,1:T(2,128)} %param.30) | data formatting | bytes 256 | tf_op args[13]
  3.3 1.5 %copy.29 = bf16[3,2,8,1024]{3,2,0,1:T(8,128)(2,1)} copy(bf16[3,2,8,1024]{3,2,1,0:T(8,128)(2,1)} %bitcast.10) | data formatting | bytes 196608 | tf_op jit(solution)/shard_map/reshape | solution.py:532
  4.9 78.6 %layer.1 = (bf16[16,1024]{1,0:T(8,128)(2,1)}, f32[16,1024]{1,0:T(8,128)}, bf16[16,3072]{1,0:T(8,128)(2,1)}) custom-call(bf16[16,1024]{1,0:T(8,128)(2,1)} %stream.1, f32[16,1024]{1,0:T(8,128)} %hidden.1, bf16[16,3072]{1,0:T(8,128)(2,1)} %bitcast.9, f32[1,1024]{1,0:T(1,128)} %bitcast.13, bf16[1024,128]{1,0:T(8,128)(2,1)} %win_hbm.1, ...), custom_call_target="tpu_custom_call" | custom-call | tf_op jit(solution)/shard_map/layer/pallas_call | solution.py:515
  83.5 1.5 %copy.31 = bf16[2,3,8,1024]{3,2,0,1:T(8,128)(2,1)} copy(bf16[2,3,8,1024]{3,2,1,0:T(8,128)(2,1)} %bitcast.12) | data formatting | bytes 196608 | tf_op jit(solution)/shard_map/reshape | solution.py:548
  85.0 1.4 %copy.34 = bf16[16,1024]{1,0:T(8,128)(2,1)} copy(bf16[16,1024]{1,0:T(8,128)(2,1)} %get-tuple-element.18) | data formatting | bytes 65536
  86.4 1.5 %copy.35 = f32[16,1024]{1,0:T(8,128)} copy(f32[16,1024]{1,0:T(8,128)} %get-tuple-element.19) | data formatting | bytes 131072

commit v2 on v1

--- a/solution.py
+++ b/solution.py
@@ -174,8 +174,16 @@
     sq[0, 0] = jnp.broadcast_to(jnp.sum(values * values, axis=1, keepdims=True), (rows, 128))
     lane = lax.broadcasted_iota(jnp.int32, (rows, 128), 1)
     wrow = jnp.zeros((rows, 128), f32)
-    for k in range(routes.shape[1]):
-        wrow += jnp.where(lane == routes[:, k : k + 1], rweight[:, k : k + 1], 0.0)
+    eye = lax.broadcasted_iota(jnp.int32, (rows, rows), 0) == lax.broadcasted_iota(
+        jnp.int32, (rows, rows), 1
+    )
+
+    def column(row):
+        return jnp.sum(jnp.where(eye, row, 0.0), axis=1, keepdims=True)
+
+    for k in range(routes.shape[0]):
+        named = column(routes[k : k + 1, :].astype(f32))
+        wrow += jnp.where(lane.astype(f32) == named, column(rweight[k : k + 1, :]), 0.0)
     wx[0, z] = wrow
 
     def weights_out():
@@ -282,11 +290,11 @@
     width = taps.shape[0]
     acc = forward.astype(f32) * taps[width - 1 : width, :].astype(f32)
     for k in range(width - 1):
-        acc += conv[:, k * half : (k + 1) * half].astype(f32) * taps[k : k + 1, :].astype(f32)
+        acc += conv[k].astype(f32) * taps[k : k + 1, :].astype(f32)
     conv_out = acc.astype(bf16)
-    if width > 2:
-        new_conv[:, : (width - 2) * half] = conv[:, half : (width - 1) * half]
-    new_conv[:, (width - 2) * half :] = forward
+    for k in range(width - 2):
+        new_conv[k] = conv[k + 1]
+    new_conv[width - 2] = forward
     groups, gw, _ = rdiag.shape
 
     def block_map(table):
@@ -428,6 +436,12 @@
     finish2()
     for c in pending:
         c.wait_send()
+
+
+def hand_over(a, b, c, x, y, z):
+    x[...] = a[...]
+    y[...] = b[...]
+    z[...] = c[...]
 
 
 def per_device(
@@ -518,7 +532,7 @@
         out_shape=(
             jax.ShapeDtypeStruct(stream.shape, bf16),
             jax.ShapeDtypeStruct(stream.shape, f32),
-            jax.ShapeDtypeStruct((rows, past * half), bf16),
+            jax.ShapeDtypeStruct((past, rows, half), bf16),
         ),
         in_specs=[v, v, v, v, a, a, v, v, v, v, a, v, v, v, a, a, a],
         out_specs=(v, v, v),
@@ -529,7 +543,7 @@
     )(
         stream,
         hidden_state,
-        conv_state.reshape(rows, past * half),
+        conv_state.transpose(1, 0, 2),
         first_gain.reshape(1, half),
         input_weight,
         branch_weight,
@@ -539,13 +553,20 @@
         decay_logit.reshape(1, half),
         output_weight,
         second_gain.reshape(1, half),
-        routes,
-        route_weight,
+        routes.T,
+        route_weight.T,
         expert_gate,
         expert_up,
         expert_down,
     )
-    return new_stream, new_hidden, new_conv.reshape(rows, past, half)
+    new_stream, new_hidden, new_conv = pl.pallas_call(
+        hand_over,
+        name="hand_over",
+        out_shape=tuple(jax.ShapeDtypeStruct(x.shape, x.dtype) for x in (new_stream, new_hidden, new_conv)),
+        in_specs=[v] * 3,
+        out_specs=(v,) * 3,
+    )(new_stream, new_hidden, new_conv)
+    return new_stream, new_hidden, new_conv.transpose(1, 0, 2)
 
 
 def solution(mesh):

time: 88.2 us -> 81.1 us (0.920)
  local copies, waits for them, and re-layouts: 8.63 us -> 0 us
  Pallas kernels: 78.6 us -> 80.2 us
    unnamed x4 -> x0, local copies, waits for them, and re-layouts: 5.55 us -> none
    reshape x2 -> x0, local copies, waits for them, and re-layouts: 3.08 us -> none  [the longest x1 1.54 us: per_device(): return (new_stream, new_hidden, new_conv.reshape(rows, past, half))]
    pallas_call x0 -> x1, Pallas kernels: none -> 1.63 us  [per_device(): pl.pallas_call(hand_over, name='hand_over', out_shape=tuple((jax.ShapeDty...]
where the time goes in v2:
time: 81.1 us; the launch traced here: 80.9 us
  Pallas kernels  80.2 us (99%)
    pallas_call x1, Pallas kernels, per_device(): pl.pallas_call(functools.partial(kernel, n), name='layer', out_shape=(jax...  78.6 us
    pallas_call x1, Pallas kernels, per_device(): pl.pallas_call(hand_over, name='hand_over', out_shape=tuple((jax.ShapeDty...  1.63 us

profile of v2, /device:TPU:0, one launch (start us, length us, event | category | flops | bytes accessed | tf_op | source)
XLA Modules:
  0.0 80.9 jit_solution(14696378676214198413)
XLA Ops:
  0.6 78.6 %layer.1 = (bf16[16,1024]{1,0:T(8,128)(2,1)}, f32[16,1024]{1,0:T(8,128)}, bf16[3,16,1024]{2,1,0:T(8,128)(2,1)}) custom-call(bf16[16,1024]{1,0:T(8,128)(2,1)} %stream.1, f32[16,1024]{1,0:T(8,128)} %hidden.1, bf16[3,16,1024]{2,1,0:T(8,128)(2,1)} %bitcast.7, f32[1,1024]{1,0:T(1,128)} %bitcast.8, bf16[1024,128]{1,0:T(8,128)(2,1)} %win_hbm.1, ...), custom_call_target="tpu_custom_call" | custom-call | tf_op jit(solution)/shard_map/layer/pallas_call | solution.py:529
  79.3 1.6 %hand_over.1 = (bf16[16,1024]{1,0:T(8,128)(2,1)}, f32[16,1024]{1,0:T(8,128)}, bf16[3,16,1024]{2,1,0:T(8,128)(2,1)}) custom-call(bf16[16,1024]{1,0:T(8,128)(2,1)} %get-tuple-element.9.a, f32[16,1024]{1,0:T(8,128)} %get-tuple-element.10.b, bf16[3,16,1024]{2,1,0:T(8,128)(2,1)} %get-tuple-element.11.c), custom_call_target="tpu_custom_call" | custom-call | tf_op jit(solution)/shard_map/hand_over/pallas_call | solution.py:562

commit v3 on v2

--- a/solution.py
+++ b/solution.py
@@ -19,26 +19,41 @@
 
 def kernel(
     n,
+    stream_hbm,
+    hidden_hbm,
+    conv_hbm,
+    gain1_hbm,
+    win_hbm,
+    wbr_hbm,
+    taps_hbm,
+    rgate_hbm,
+    igate_hbm,
+    decay_hbm,
+    wout_hbm,
+    gain2_hbm,
+    routes_hbm,
+    rweight_hbm,
+    wg_hbm,
+    wu_hbm,
+    wd_hbm,
+    new_stream_hbm,
+    new_hidden_hbm,
+    new_conv_hbm,
     stream,
     hidden,
     conv,
     gain1,
-    win_hbm,
-    wbr_hbm,
     taps,
     rgate,
     igate,
     decay,
-    wout_hbm,
     gain2,
     routes,
     rweight,
-    wg_hbm,
-    wu_hbm,
-    wd_hbm,
     new_stream,
     new_hidden,
     new_conv,
+    out_sem,
     win,
     wbr,
     wout,
@@ -116,58 +131,122 @@
         pending.append(c)
         return c
 
-    loads = []
-    for i, (a, b) in enumerate(
-        ((win_hbm, win), (wbr_hbm, wbr), (wout_hbm, wout), (wg_hbm, wg), (wu_hbm, wu), (wd_hbm, wd))
-    ):
+    barrier = pltpu.get_barrier_semaphore()
+    pl.semaphore_signal(barrier, inc=1, device_id=(e, other), device_id_type=MESH)
+
+    @pl.loop(1, n)
+    def _(d):
+        peer = lax.rem(e + d, n)
+        pl.semaphore_signal(barrier, inc=1, device_id=(peer, t), device_id_type=MESH)
+        pl.semaphore_signal(barrier, inc=1, device_id=(peer, other), device_id_type=MESH)
+
+    def load(i, a, b):
         c = pltpu.make_async_copy(a, b, load_sem.at[i])
         c.start()
-        loads.append(c)
+        return c
+
+    firsts = [
+        load(6 + i, a, b)
+        for i, (a, b) in enumerate(
+            ((stream_hbm, stream), (gain1_hbm, gain1), (routes_hbm, routes), (rweight_hbm, rweight))
+        )
+    ]
+    loads = [load(i, a, b) for i, (a, b) in enumerate(((win_hbm, win), (wbr_hbm, wbr)))]
+    smalls = [
+        load(10 + i, a, b)
+        for i, (a, b) in enumerate(
+            (
+                (rgate_hbm, rgate),
+                (igate_hbm, igate),
+                (hidden_hbm, hidden),
+                (conv_hbm, conv),
+                (taps_hbm, taps),
+                (decay_hbm, decay),
+                (gain2_hbm, gain2),
+            )
+        )
+    ]
+    loads += [
+        load(2 + i, a, b)
+        for i, (a, b) in enumerate(((wout_hbm, wout), (wg_hbm, wg), (wu_hbm, wu), (wd_hbm, wd)))
+    ]
+    for c in firsts:
+        c.wait()
+
+    near = [sorted(range(zn), key=lambda o: (abs(o - i), o)) for i in range(zn)]
+    at = [z]
+    for j in range(1, zn):
+        pick = near[0][j]
+        for i in range(1, zn):
+            pick = jnp.where(z == i, near[i][j], pick)
+        at.append(pick)
+    ed = ex + ey - e
+    held = max(2, zn // 2)
 
     def gather(buf, p, after=None):
         s, r = ag_s.at[p], ag_r.at[p]
-        at = [lax.rem(z - k + zn, zn) for k in range(zn)]
-        zc = [None] * zn
-        for k in range(1, zn):
-            target = lax.rem(e + PLANE * k, n)
-            zc[k] = send(buf.at[0, z], buf.at[0, z], s.at[0, k], r.at[0, k], target, t)
-        xc, yc, dc = [None] * zn, [None] * zn, [None] * zn
-
-        def diagonal(k):
-            if k % 2 == 0:
-                xc[k].wait_recv()
-                dc[k] = send(buf.at[1, at[k]], buf.at[3, at[k]], s.at[3, k], r.at[3, k], ey, t)
+        zc, xc, yc, dc = [], [], [], []
+
+        def line(j, peer):
+            return rcopy(
+                buf.at[0, z], buf.at[0, z], s.at[0, peer], r.at[0, z], peer * PLANE + low, t
+            )
+
+        for j in range(1, zn):
+            c = line(j, at[j])
+            c.start()
+            zc.append(c)
+        pending.extend(zc)
+
+        def pass_on(j):
+            a = at[j]
+            xc.append(send(buf.at[0, a], buf.at[1, a], s.at[1, a], r.at[1, a], ex, t))
+            yc.append(send(buf.at[0, a], buf.at[2, a], s.at[2, a], r.at[2, a], ey, t))
+            if j >= held:
+                dc.append(send(buf.at[0, a], buf.at[3, a], s.at[3, a], r.at[3, a], ed, t))
+
+        def relayed(j):
+            a = at[j]
+            if j % 2 == 0:
+                xc[j].wait_recv()
+                dc.append(send(buf.at[1, a], buf.at[3, a], s.at[3, a], r.at[3, a], ey, t))
+            else:
+                yc[j].wait_recv()
+                dc.append(send(buf.at[2, a], buf.at[3, a], s.at[3, a], r.at[3, a], ex, t))
+            if after:
+                after(1 + j % 2, a)
+
+        for j in range(zn):
+            a = at[j]
+            if j:
+                rcopy(buf.at[0, a], buf.at[0, a], s.at[0, a], r.at[0, a], e, other).wait_recv()
+            pass_on(j)
+            if after:
+                after(0, a)
+            if 1 <= j <= held:
+                relayed(j - 1)
+        for j in range(zn):
+            a = at[j]
+            if j >= held:
+                xc[j].wait_recv()
                 if after:
-                    after(1, at[k], k)
+                    after(1, a)
+                yc[j].wait_recv()
+                if after:
+                    after(2, a)
+            elif j % 2 == 0:
+                yc[j].wait_recv()
+                if after:
+                    after(2, a)
             else:
-                yc[k].wait_recv()
-                dc[k] = send(buf.at[2, at[k]], buf.at[3, at[k]], s.at[3, k], r.at[3, k], ex, t)
+                xc[j].wait_recv()
                 if after:
-                    after(2, at[k], k)
-
-        for k in range(zn):
-            if k:
-                zc[k].wait_recv()
-            xc[k] = send(buf.at[0, at[k]], buf.at[1, at[k]], s.at[1, k], r.at[1, k], ex, t)
-            yc[k] = send(buf.at[0, at[k]], buf.at[2, at[k]], s.at[2, k], r.at[2, k], ey, t)
+                    after(1, a)
+        for j in range(zn):
+            a = at[j]
+            rcopy(buf.at[0, a], buf.at[3, a], s.at[3, a], r.at[3, a], e, other).wait_recv()
             if after:
-                after(0, at[k], k)
-            if k:
-                diagonal(k - 1)
-        diagonal(zn - 1)
-        for k in range(zn):
-            if k % 2 == 0:
-                yc[k].wait_recv()
-                if after:
-                    after(2, at[k], k)
-            else:
-                xc[k].wait_recv()
-                if after:
-                    after(1, at[k], k)
-        for k in range(zn):
-            dc[k].wait_recv()
-            if after:
-                after(3, at[k], k)
+                after(3, a)
 
     values = stream[...].astype(f32)
     x1[0, z] = (values * gain1[...]).astype(bf16)
@@ -198,6 +277,7 @@
                 out.append(send(wx.at[0, z], wx.at[q, z], wx_s.at[q, k], wx_r.at[q, k], target, t))
         return out
 
+    pl.semaphore_wait(barrier, 2 * n - 1)
     sq1 = send(sq.at[0, 0], sq.at[0, 1], sq_s.at[0], sq_r.at[0], e, other)
 
     def prepare():
@@ -212,6 +292,8 @@
 
     gather(x1, 0)
     wxc = weights_out()
+    for c in smalls:
+        c.wait()
     prepare()
 
     loads[0].wait()
@@ -318,9 +400,15 @@
         inward * conv_out.astype(f32)
     )
     new_hidden[...] = state
+    outs = [
+        pltpu.make_async_copy(a, b, out_sem.at[i])
+        for i, (a, b) in enumerate(((new_hidden, new_hidden_hbm), (new_conv, new_conv_hbm)))
+    ]
     gelu = 0.5 * branch * (1.0 + jnp.tanh(0.7978845608028654 * (branch + 0.044715 * branch * branch * branch)))
     x2[0, z] = (gelu * state).astype(bf16)
 
+    for c in outs:
+        c.start()
     gather(x2, 1)
     loads[2].wait()
     (osum,), finish2 = project(x2, (wout,), pair2s, pair2r, fin2, y2, 1)
@@ -333,10 +421,8 @@
 
     xpc = []
 
-    def relay(q, at, k):
-        xpc.append(
-            send(x3.at[q, at], xp.at[q, at], xp_s.at[q, k], xp_r.at[q, k], e, other)
-        )
+    def relay(q, a):
+        xpc.append(send(x3.at[q, a], xp.at[q, a], xp_s.at[q, a], xp_r.at[q, a], e, other))
 
     gather(x3, 2, relay)
     loads[3].wait()
@@ -376,41 +462,41 @@
 
     each(PLANE // step, experts)
 
-    def row_weights(qs):
-        full = wx[qs].reshape(step * mrows, 128)
+    hw = half // 2
+
+    def weights_of(q):
+        full = wx[q].reshape(mrows, 128)
         lanes = lax.broadcasted_iota(jnp.int32, full.shape, 1)
         return jnp.sum(jnp.where(lanes == expert, full, 0.0), axis=1, keepdims=True)
 
-    hw = half // 2
-
-    def store(ref, qs, lanes):
-        def run():
-            act = inner[qs].reshape(step * mrows, inner.shape[2])
-            out = jnp.dot(act, wd[:, lanes], preferred_element_type=f32) * row_weights(qs)
-            for i in range(2):
-                ref[i, qs] = (
-                    out[:, i * hw : (i + 1) * hw].astype(ref.dtype).reshape(step, zn, rows, hw)
-                )
-
-        return run
-
-    each(PLANE // step, lambda c: store(pair3s, pl.ds(c * step, step), there)())
-    pc = send(pair3s, pair3r, pair_s.at[2], pair_r.at[2], e, other)
-    each(PLANE // step, lambda c: store(keep, pl.ds(c * step, step), here)())
-    pc.wait_recv()
+    def down(ref, q, lanes):
+        out = jnp.dot(inner[q], wd[:, lanes], preferred_element_type=f32) * weights_of(q)
+        for i in range(2):
+            ref[q, i] = out[:, i * hw : (i + 1) * hw].astype(ref.dtype).reshape(zn, rows, hw)
+
+    pcs = {}
+    for q in (3, 1, 2, 0):
+        down(pair3s, q, there)
+        pcs[q] = send(pair3s.at[q], pair3r.at[q], pair_s.at[2 + q], pair_r.at[2 + q], e, other)
+    for q in (3, 1, 2, 0):
+        down(keep, q, here)
 
     def total(i, q):
-        return keep[i, q] + pair3r[i, q].astype(f32)
+        return keep[q, i] + pair3r[q, i].astype(f32)
 
     first = (1, 2)
     rc = [[None, None], [None, None]]
     peers = (ex, ey)
+    pcs[3].wait_recv()
     for i in range(2):
         sums[i, 1] = total(i, 3).astype(bf16)
         rc[i][1] = send(sums.at[i, 1], r1.at[i, 1], rs_s.at[0, i, 1], rs_r.at[0, i, 1], peers[i], t)
+    pcs[1].wait_recv()
+    pcs[2].wait_recv()
     for i in range(2):
         sums[i, 0] = total(i, first[i]).astype(bf16)
         rc[i][0] = send(sums.at[i, 0], r1.at[i, 0], rs_s.at[0, i, 0], rs_r.at[0, i, 0], peers[i], t)
+    pcs[0].wait_recv()
     sc = [None, None]
     for i in range(2):
         rc[i][1].wait_recv()
@@ -419,23 +505,27 @@
     for i in range(2):
         rc[i][0].wait_recv()
         sc[i].wait_recv()
-        keep[i, 0] = total(i, 0) + r1[i, 0].astype(f32) + r2[i].astype(f32)
-        u3[:, :, i * hw : (i + 1) * hw] = keep[i, 0].astype(bf16)
+        keep[0, i] = total(i, 0) + r1[i, 0].astype(f32) + r2[i].astype(f32)
+        u3[:, :, i * hw : (i + 1) * hw] = keep[0, i].astype(bf16)
     zc = []
     for k in range(1, zn):
         dest = lax.rem(z + k, zn)
         zc.append(
             send(u3.at[dest], r3.at[k], rs_s.at[2, 0, k], rs_r.at[2, 0, k], dest * PLANE + low, t)
         )
-    mix = jnp.concatenate([keep[0, 0, z], keep[1, 0, z]], axis=1)
+    mix = jnp.concatenate([keep[0, 0, z], keep[0, 1, z]], axis=1)
     for k in range(1, zn):
         zc[k - 1].wait_recv()
         mix += r3[k].astype(f32)
     new_stream[...] = (middle + mix).astype(bf16)
+    outs.append(pltpu.make_async_copy(new_stream, new_stream_hbm, out_sem.at[2]))
+    outs[2].start()
     finish1()
     finish2()
     for c in pending:
         c.wait_send()
+    for c in outs:
+        c.wait()
 
 
 def hand_over(a, b, c, x, y, z):
@@ -476,7 +566,23 @@
     vm = pltpu.VMEM
     any_spec = pl.BlockSpec(memory_space=pl.ANY)
     vspec = pl.BlockSpec(memory_space=pltpu.VMEM)
+    top = routes.shape[1]
     scratch = [
+        vm(stream.shape, bf16),
+        vm(stream.shape, f32),
+        vm((past, rows, half), bf16),
+        vm((1, half), f32),
+        vm(conv_taps.shape, bf16),
+        vm(recur_gate.shape, bf16),
+        vm(input_gate.shape, bf16),
+        vm((1, half), f32),
+        vm((1, half), f32),
+        vm((top, rows), jnp.int32),
+        vm((top, rows), f32),
+        vm(stream.shape, bf16),
+        vm(stream.shape, f32),
+        vm((past, rows, half), bf16),
+        dma((3,)),
         vm(input_weight.shape, bf16),
         vm(branch_weight.shape, bf16),
         vm(output_weight.shape, bf16),
@@ -500,24 +606,24 @@
         vm((hn, 1, rows, cols), bf16),
         vm((hn, 1, rows, cols), bf16),
         vm((PLANE, zn * rows, hidden_units), bf16),
-        vm((2, PLANE, zn, rows, hw), bf16),
-        vm((2, PLANE, zn, rows, hw), bf16),
-        vm((2, PLANE, zn, rows, hw), f32),
+        vm((PLANE, 2, zn, rows, hw), bf16),
+        vm((PLANE, 2, zn, rows, hw), bf16),
+        vm((PLANE, 2, zn, rows, hw), f32),
         vm((2, 2, zn, rows, hw), bf16),
         vm((2, 2, zn, rows, hw), bf16),
         vm((2, zn, rows, hw), bf16),
         vm((2, zn, rows, hw), bf16),
         vm((zn, rows, half), bf16),
         vm((zn, rows, half), bf16),
-        dma((6,)),
+        dma((17,)),
         dma((PLANE, zn)),
         dma((PLANE, zn)),
         dma((2,)),
         dma((2,)),
         dma((3, PLANE, zn)),
         dma((3, PLANE, zn)),
-        dma((3,)),
-        dma((3,)),
+        dma((6,)),
+        dma((6,)),
         dma((2, hn)),
         dma((2, hn)),
         dma((PLANE, zn)),
@@ -534,11 +640,11 @@
             jax.ShapeDtypeStruct(stream.shape, f32),
             jax.ShapeDtypeStruct((past, rows, half), bf16),
         ),
-        in_specs=[v, v, v, v, a, a, v, v, v, v, a, v, v, v, a, a, a],
-        out_specs=(v, v, v),
+        in_specs=[a] * 17,
+        out_specs=(a, a, a),
         scratch_shapes=scratch,
         compiler_params=pltpu.CompilerParams(
-            has_side_effects=True, vmem_limit_bytes=60 * 1024 * 1024
+            collective_id=0, has_side_effects=True, vmem_limit_bytes=60 * 1024 * 1024
         ),
     )(
         stream,

time: 81.1 us -> 71.2 us (0.88)
  Pallas kernels: 80.2 us -> 70.4 us
    pallas_call x1, Pallas kernels: 78.6 us -> 68.8 us  [per_device(): pl.pallas_call(functools.partial(kernel, n), name='layer', out_shape=(jax...]
where the time goes in v3:
time: 71.2 us; the launch traced here: 71 us
  Pallas kernels  70.4 us (99%)
    pallas_call x1, Pallas kernels, per_device(): pl.pallas_call(functools.partial(kernel, n), name='layer', out_shape=(jax...  68.8 us
    pallas_call x1, Pallas kernels, per_device(): pl.pallas_call(hand_over, name='hand_over', out_shape=tuple((jax.ShapeDty...  1.63 us

profile of v3, /device:TPU:0, one launch (start us, length us, event | category | flops | bytes accessed | tf_op | source)
XLA Modules:
  0.0 71.0 jit_solution(18404333853800010074)
XLA Ops:
  0.6 68.8 %layer.1 = (bf16[16,1024]{1,0:T(8,128)(2,1)}, f32[16,1024]{1,0:T(8,128)}, bf16[3,16,1024]{2,1,0:T(8,128)(2,1)}) custom-call(bf16[16,1024]{1,0:T(8,128)(2,1)} %stream_hbm.1, f32[16,1024]{1,0:T(8,128)} %hidden_hbm.1, bf16[3,16,1024]{2,1,0:T(8,128)(2,1)} %bitcast.7, f32[1,1024]{1,0:T(1,128)} %bitcast.8, bf16[1024,128]{1,0:T(8,128)(2,1)} %win_hbm.1, ...), custom_call_target="tpu_custom_call" | custom-call | tf_op jit(solution)/shard_map/layer/pallas_call | solution.py:635
  69.4 1.6 %hand_over.1 = (bf16[16,1024]{1,0:T(8,128)(2,1)}, f32[16,1024]{1,0:T(8,128)}, bf16[3,16,1024]{2,1,0:T(8,128)(2,1)}) custom-call(bf16[16,1024]{1,0:T(8,128)(2,1)} %get-tuple-element.9.a, f32[16,1024]{1,0:T(8,128)} %get-tuple-element.10.b, bf16[3,16,1024]{2,1,0:T(8,128)(2,1)} %get-tuple-element.11.c), custom_call_target="tpu_custom_call" | custom-call | tf_op jit(solution)/shard_map/hand_over/pallas_call | solution.py:668
